TPU v7x, 32 devices: a whole 2x2x4 slice. The times are simulated.
32 devices in a mesh: fs: 8 (over z, y), tp: 4 (over x, core).
Axes of the slice: x: 2, y: 2, z: 4, core: 2. Of those that a mesh axis runs over, the one named last changes fastest.
Arguments:
- inputs: bfloat16 [16384, 2048], P('fs'), may hold values from -6 to 6
- attn_out: bfloat16 [16384, 1024], P('fs', 'tp'), may hold values from -6 to 6
- grad_query: bfloat16 [16384, 1024], P('fs', 'tp'), may hold values from -0.125 to 0.125
- grad_key: bfloat16 [16384, 1024], P('fs', 'tp'), may hold values from -0.125 to 0.125
- grad_mixed: bfloat16 [16384, 2048], P('fs'), may hold values from -0.15625 to 0.15625
- query_weight: float32 [2048, 1024], P('fs', 'tp'), may hold values from -0.75 to 0.75
- key_weight: float32 [2048, 1024], P('fs', 'tp'), may hold values from -0.75 to 0.75
- out_weight: float32 [1024, 2048], P('tp', 'fs'), may hold values from -0.75 to 0.75
- factors: bfloat16 [3, 2048, 256], P(None, 'fs'), may hold values from -0.125 to 0.125
- moment_first: float32 [3, 256, 1024], P(None, 'fs', 'tp'), may hold values from -6 to 6
- moment_second: float32 [3, 256, 1024], P(None, 'fs', 'tp'), may hold values from 0.05 to 2
Outputs:
- step_query: float32 [2048, 1024], P('fs', 'tp')
- step_key: float32 [2048, 1024], P('fs', 'tp')
- step_out: float32 [1024, 2048], P('tp', 'fs')
- copy_query: bfloat16 [2048, 1024], P(None, 'tp')
- copy_key: bfloat16 [2048, 1024], P(None, 'tp')
- copy_out: bfloat16 [1024, 2048], P('tp')
- first_new: float32 [3, 256, 1024], P(None, 'fs', 'tp')
- second_new: float32 [3, 256, 1024], P(None, 'fs', 'tp')
All inputs are finite; a program needn't handle non-finite values.
Results may differ from a plain program's by a relative error of at most 0.006.
Values may be sent and summed in bfloat16 or wider, within the bound.
A program may use at most 128 MiB of HBM per device.

v0:
```python
import jax
import jax.numpy as jnp
from jax import lax
from jax.sharding import PartitionSpec as P

RANK = 256
HW = 1024


first_decay = 0.8
second_decay = 0.9
epsilon = 1e-08
learn_rate = 0.02


def over_tokens(left_side, right_side):
    return jnp.dot(left_side.T, right_side, preferred_element_type=jnp.float32)


def moments_update(projected, old_first, old_second):
    first_new = first_decay * old_first + (1.0 - first_decay) * projected
    second_new = second_decay * old_second + (1.0 - second_decay) * projected * projected
    adam_ratio = first_new / (jnp.sqrt(second_new) + epsilon)
    return (first_new, second_new, adam_ratio)


def per_device(
    inputs,
    attn_out,
    grad_query,
    grad_key,
    grad_mixed,
    query_weight,
    key_weight,
    out_weight,
    factors,
    moment_first,
    moment_second,
):
    pairs = ((inputs, grad_query), (inputs, grad_key), (grad_mixed, attn_out))
    partial_value = []
    whole_factors = lax.all_gather(factors, "fs", axis=1, tiled=True)
    for matrix_number in range(3):
        left_side, right_side = pairs[matrix_number]
        mapped = jnp.dot(
            left_side, whole_factors[matrix_number], preferred_element_type=jnp.float32
        )
        upper_part = mapped.astype(jnp.bfloat16)
        lower_part = (mapped - upper_part.astype(jnp.float32)).astype(jnp.bfloat16)
        partial_value.append(
            over_tokens(upper_part, right_side) + over_tokens(lower_part, right_side)
        )
    partial_sums = jnp.stack(partial_value)
    reduced = lax.psum_scatter(partial_sums, "fs", scatter_dimension=1, tiled=True)
    first_new, second_new, adam_ratio = moments_update(reduced, moment_first, moment_second)
    square_total = lax.psum(jnp.sum(adam_ratio * adam_ratio), ("fs", "tp"))
    directions = lax.all_gather(adam_ratio.astype(jnp.bfloat16), "fs", axis=1, tiled=True)
    step_scale = lax.rsqrt(square_total / (3 * RANK * HW) + 1.0)
    step_query = step_scale * jnp.dot(factors[0], directions[0], preferred_element_type=jnp.float32)
    step_key = step_scale * jnp.dot(factors[1], directions[1], preferred_element_type=jnp.float32)
    step_out = step_scale * jnp.dot(factors[2], directions[2], preferred_element_type=jnp.float32).T
    new_query = (query_weight - learn_rate * step_query).astype(jnp.bfloat16)
    new_key = (key_weight - learn_rate * step_key).astype(jnp.bfloat16)
    new_out = (out_weight - learn_rate * step_out).astype(jnp.bfloat16)
    copy_query, copy_key, copy_out = (
        lax.all_gather(new_query, "fs", axis=0, tiled=True),
        lax.all_gather(new_key, "fs", axis=0, tiled=True),
        lax.all_gather(new_out, "fs", axis=1, tiled=True),
    )
    return (step_query, step_key, step_out, copy_query, copy_key, copy_out, first_new, second_new)


def solution(mesh):
    in_specs = (
        P("fs", None),
        P("fs", "tp"),
        P("fs", "tp"),
        P("fs", "tp"),
        P("fs", None),
        P("fs", "tp"),
        P("fs", "tp"),
        P("tp", "fs"),
        P(None, "fs", None),
        P(None, "fs", "tp"),
        P(None, "fs", "tp"),
    )
    out_specs = (
        P("fs", "tp"),
        P("fs", "tp"),
        P("tp", "fs"),
        P(None, "tp"),
        P(None, "tp"),
        P("tp", None),
        P(None, "fs", "tp"),
        P(None, "fs", "tp"),
    )
    return jax.shard_map(
        per_device, mesh=mesh, in_specs=in_specs, out_specs=out_specs, check_vma=False
    )
```

profile of v0, /device:TPU:0, one launch (start us, length us, event | category | flops | bytes accessed | tf_op | source)
XLA Modules:
  0.0 357.2 jit_solution(18089917660759252237)
XLA Ops:
  7.2 0.7 all-gather.5.cloned.1.call-update
  8.0 65.0 %all-gather.5.cloned.1.call-done = bf16[3,2048,256]{2,1,0:T(8,128)(2,1)} async-done(((bf16[3,256,256]{2,1,0:T(8,128)(2,1)}), bf16[3,2048,256]{2,1,0:T(8,128)(2,1)}) %all-gather.5.cloned.1.call-update) | async-done | bytes 3145744 | tf_op jit(solution)/shard_map/all_gather | solution.py:42
  73.0 6.2 %fusion.6 = f32[2048,256]{1,0:T(8,128)S(1)} fusion(bf16[2048,2048]{1,0:T(8,128)(2,1)} %param.11, bf16[3,2048,256]{2,1,0:T(8,128)(2,1)} %all-gather.5.cloned.1.call-done), kind=kOutput, calls=%fused_computation.17 | convolution fusion | flops 2147483648 | bytes 11534336 | tf_op jit(solution)/shard_map/dot_general | solution.py:45
  79.2 0.5 fusion.12
  79.7 0.5 fusion.3
  80.2 0.9 copy-done.13
  81.1 2.4 fusion.7
  84.6 2.4 fusion.5
  88.1 0.9 pad_maximum_fusion
  89.2 62.6 %reduce-scatter.2.cloned.1.call-done = f32[3,32,256]{2,1,0:T(8,128)} async-done(((f32[3,256,256]{2,1,0:T(8,128)}), f32[3,32,256]{2,1,0:T(8,128)}) %reduce-scatter.2.cloned.1.call-update) | async-done | bytes 98320 | tf_op jit(solution)/shard_map/reduce_scatter | solution.py:54
  151.8 1.6 multiply_reduce_fusion
  153.4 31.2 %all_gather.16 = bf16[3,256,256]{2,1,0:T(8,128)(2,1)S(1)} all-gather(bf16[3,32,256]{2,1,0:T(8,128)(2,1)S(1)} %fusion.24), channel_id=1, replica_groups=mesh['fs'=8,'tp'=4] {'fs'}, dimensions={1}, use_global_device_ids=true | all-gather | bytes 442368 | tf_op jit(solution)/shard_map/all_gather | solution.py:57
  184.6 37.6 %psum.7 = f32[]{:T(128)} all-reduce(f32[]{:T(128)} %get-tuple-element.16), channel_id=1, replica_groups=mesh['fs'=8,'tp'=4] {'fs','tp'}, use_global_device_ids=true, to_apply=%region_2.0 | all-reduce | flops 1 | bytes 8 | tf_op jit(solution)/shard_map/psum | solution.py:56
  222.9 0.8 subtract_convert_fusion.6
  223.8 0.9 subtract_convert_fusion.7
  225.0 0.9 subtract_convert_fusion.8
  225.9 0.8 copy.26
  226.8 0.8 copy.25
  227.6 37.6 %all-gather.11.cloned.1.call-done = bf16[256,2048]{0,1:T(8,128)(2,1)} async-done(((bf16[256,256]{0,1:T(8,128)(2,1)}), bf16[256,2048]{0,1:T(8,128)(2,1)}) %all-gather.11.cloned.1.call-update) | async-done | bytes 1048592 | tf_op jit(solution)/shard_map/all_gather | solution.py:68
  265.2 2.3 copy.28
  267.5 39.3 %all-gather.9.cloned.1.call-done = bf16[2048,256]{1,0:T(8,128)(2,1)} async-done(((bf16[256,256]{1,0:T(8,128)(2,1)}), bf16[2048,256]{1,0:T(8,128)(2,1)}) %all-gather.9.cloned.1.call-update) | async-done | bytes 1048592 | tf_op jit(solution)/shard_map/all_gather | solution.py:67
  306.8 40.6 %all-gather.7.cloned.1.call-done = bf16[2048,256]{0,1:T(8,128)(2,1)} async-done(((bf16[256,256]{0,1:T(8,128)(2,1)}), bf16[2048,256]{0,1:T(8,128)(2,1)}) %all-gather.7.cloned.1.call-update) | async-done | bytes 1048592 | tf_op jit(solution)/shard_map/all_gather | solution.py:66
  347.4 2.3 copy.27
  349.7 1.0 copy.32
  (48 shorter events, 2.5 us)
Async XLA Ops:
  7.2 72.0 %copy-start = (bf16[2048,256]{1,0:T(8,128)(2,1)S(1)}, bf16[2048,256]{1,0:T(8,128)(2,1)}, u32[]{:S(2)}) copy-start(bf16[2048,256]{1,0:T(8,128)(2,1)} %param.14) | copy-start | bytes 3145732
  7.2 65.8 %all-gather.5.cloned.1.call-start = ((), (), s32[]{:S(2)}) async-start(), calls=%async_computation.1 | async-start | bytes 3538944 | tf_op jit(solution)/shard_map/all_gather | solution.py:42
  7.9 143.9 %reduce-scatter.2.cloned.1.call-start = ((), (), s32[]{:S(2)}) async-start(), calls=%async_computation.2 | async-start | bytes 884736 | tf_op jit(solution)/shard_map/reduce_scatter | solution.py:54
  73.0 7.3 %copy-start.12 = (bf16[2048,2048]{1,0:T(8,128)(2,1)S(1)}, bf16[2048,2048]{1,0:T(8,128)(2,1)}, u32[]{:S(2)}) copy-start(bf16[2048,2048]{1,0:T(8,128)(2,1)} %param.11) | copy-start | bytes 25165828
  79.2 1.9 copy-start.13
  79.7 4.8 %slice-start = ((s8[8388608]{0:T(1024)(128)(4,1)}), s8[4194304]{0:T(1024)(128)(4,1)S(1)}, s32[]{:S(2)}) async-start(s8[8388608]{0:T(1024)(128)(4,1)} %bitcast.58), calls=%async_computation.6 | async-start | bytes 8388608
  81.1 2.5 copy-start.1
  81.1 3.4 slice-start.1
  84.6 2.5 copy-start.2
  88.0 1.1 copy-start.8
  88.0 63.8 %copy-start.10 = (f32[3,32,256]{2,1,0:T(8,128)S(1)}, f32[3,32,256]{2,1,0:T(8,128)}, u32[]{:S(2)}) copy-start(f32[3,32,256]{2,1,0:T(8,128)} %param.21) | copy-start | bytes 294916
  88.0 63.8 %copy-start.11 = (f32[3,32,256]{2,1,0:T(8,128)S(1)}, f32[3,32,256]{2,1,0:T(8,128)}, u32[]{:S(2)}) copy-start(f32[3,32,256]{2,1,0:T(8,128)} %param.20) | copy-start | bytes 294916
  88.0 134.9 %copy-start.3 = (bf16[3,256,256]{2,1,0:T(8,128)(2,1)S(1)}, bf16[3,256,256]{2,1,0:T(8,128)(2,1)}, u32[]{:S(2)}) copy-start(bf16[3,256,256]{2,1,0:T(8,128)(2,1)} %param.19) | copy-start | bytes 1179652
  89.0 134.9 %copy-start.7 = (f32[256,256]{1,0:T(8,128)S(1)}, f32[256,256]{1,0:T(8,128)}, u32[]{:S(2)}) copy-start(f32[256,256]{1,0:T(8,128)} %param.17) | copy-start | bytes 786436
  89.0 135.8 %copy-start.9 = (f32[256,256]{1,0:T(8,128)S(1)}, f32[256,256]{1,0:T(8,128)}, u32[]{:S(2)}) copy-start(f32[256,256]{1,0:T(8,128)} %param.16) | copy-start | bytes 786436
  89.0 176.2 %all-gather.11.cloned.1.call-start = ((), (), s32[]{:S(2)}) async-start(), calls=%async_computation.5 | async-start | bytes 1179648 | tf_op jit(solution)/shard_map/all_gather | solution.py:68
  153.4 72.5 %copy-start.5 = (f32[3,32,256]{2,1,0:T(8,128)}, f32[3,32,256]{2,1,0:T(8,128)S(1)}, u32[]{:S(2)}) copy-start(f32[3,32,256]{2,1,0:T(8,128)S(1)} %get-tuple-element.40) | copy-start | bytes 294916
  153.4 72.5 %copy-start.6 = (f32[3,32,256]{2,1,0:T(8,128)}, f32[3,32,256]{2,1,0:T(8,128)S(1)}, u32[]{:S(2)}) copy-start(f32[3,32,256]{2,1,0:T(8,128)S(1)} %get-tuple-element.39) | copy-start | bytes 294916
  223.8 83.0 %all-gather.9.cloned.1.call-start = ((), (), s32[]{:S(2)}) async-start(), calls=%async_computation.4 | async-start | bytes 1179648 | tf_op jit(solution)/shard_map/all_gather | solution.py:67
  224.8 122.6 %all-gather.7.cloned.1.call-start = ((), (), s32[]{:S(2)}) async-start(), calls=%async_computation.3 | async-start | bytes 1179648 | tf_op jit(solution)/shard_map/all_gather | solution.py:66
  306.8 42.9 %copy-start.4 = (bf16[2048,256]{1,0:T(8,128)(2,1)S(1)}, bf16[2048,256]{1,0:T(8,128)(2,1)}, u32[]{:S(2)}) copy-start(bf16[2048,256]{1,0:T(8,128)(2,1)} %all-gather.9.cloned.1.call-done) | copy-start | bytes 3145732
Sparse Core Ops, SparseCore 0:
  10.2 62.7 all-gather.4
  89.1 62.6 reduce-scatter.1
  223.9 41.2 all-gather.10
  267.8 38.9 all-gather.8
  309.3 38.0 all-gather.6
where the time goes:
time: 358 us; the launch traced here: 357 us
  waiting for transfers between devices  246 us (69%)
  blocking collectives  68.8 us (19%)
  matrix products  16.7 us (5%)
  between operations  14.7 us (4%)
  local copies, waits for them, and re-layouts  8.36 us (2%)
    all_gather x1, waiting for transfers between devices, per_device(): whole_factors = lax.all_gather(factors, 'fs', axis=1, tiled=True)  65 us
    reduce_scatter x1, waiting for transfers between devices, per_device(): lax.psum_scatter(partial_sums, 'fs', scatter_dimension=1, tiled=True)  62.6 us
    all_gather x1, waiting for transfers between devices, per_device(): lax.all_gather(new_query, 'fs', axis=0, tiled=True)  40.6 us
    all_gather x1, waiting for transfers between devices, per_device(): lax.all_gather(new_key, 'fs', axis=0, tiled=True)  39.3 us
    all_gather x1, waiting for transfers between devices, per_device(): lax.all_gather(new_out, 'fs', axis=1, tiled=True)  37.6 us
    psum x1, blocking collectives, per_device(): square_total = lax.psum(jnp.sum(adam_ratio * adam_ratio), ('fs', 'tp'))  37.6 us
    all_gather x1, blocking collectives, per_device(): lax.all_gather(adam_ratio.astype(jnp.bfloat16), 'fs', axis=1, tiled=True)  31.2 us
    dot_general x3, matrix products, per_device(): jnp.dot(left_side, whole_factors[matrix_number], preferred_element_type=j...  11.1 us
  transfers between devices with their start and end apart: 5, of which 5 were waited for; matrix products, arithmetic and copies ran while one was open for 2% of the time, Pallas kernels for 0%

commit v1 on v0

v1 whole, which is shorter than its diff:
```python
import functools

import jax
import jax.numpy as jnp
from jax import lax
from jax.experimental import pallas as pl
from jax.experimental.pallas import tpu as pltpu
from jax.sharding import PartitionSpec as P

MESH = pl.DeviceIdType.MESH
BF, F32 = jnp.bfloat16, jnp.float32

first_decay = 0.8
second_decay = 0.9
epsilon = 1e-08
learn_rate = 0.02
CHUNKS = 4


def flip(index, bit):
    return index + bit * (1 - 2 * ((index // bit) % 2))


def kernel(
    n, ntp,
    x_hbm, mixed_hbm, gq_ref, gk_ref, ao_ref, wq_ref, wk_ref, wo_ref, f_ref, m1_ref, m2_ref,
    fall_out, wall, r_out, scale_out, first_ref, second_ref,
    xv, gt, fall, wsrc, ps, pr, rsrc, rall, part, parts_tp, psum_fs, parts_fs,
    ld_sem, own_sem, fsend, frecv, wsend, wrecv, psend, precv, rsend, rrecv, ssend, srecv, tsend, trecv,
):
    me, q = lax.axis_index("fs"), lax.axis_index("tp")
    inner, outer = me % 2, me // 2
    nout = n // 2
    rows = f_ref.shape[1]
    rq = rows // ntp
    rk = m1_ref.shape[1]
    depth = x_hbm.shape[1]
    width = depth // CHUNKS
    bits = []
    b = ntp // 2
    while b >= 1:
        bits.append(b)
        b //= 2

    loads = []
    for a, src in enumerate((x_hbm, mixed_hbm)):
        for c in range(CHUNKS):
            cut = pl.ds(c * width, width)
            copy = pltpu.make_async_copy(src.at[:, cut], xv.at[a, :, cut], ld_sem.at[a * CHUNKS + c])
            copy.start()
            loads.append(copy)

    z_peers = [((outer + k) % nout) * 2 + inner for k in range(1, nout)]
    y_peer = me + 1 - 2 * inner
    y_side = [((outer + k) % nout) * 2 + 1 - inner for k in range(1, nout)]
    others = z_peers + [y_peer] + y_side
    tp_peers = [(q + k) % ntp for k in range(1, ntp)]

    barrier = pltpu.get_barrier_semaphore()
    for p in others:
        pl.semaphore_signal(barrier, inc=1, device_id=(p, q), device_id_type=MESH)
    for t in tp_peers:
        pl.semaphore_signal(barrier, inc=1, device_id=(me, t), device_id_type=MESH)
    pl.semaphore_wait(barrier, len(others) + len(tp_peers))

    def remote(src, dst, send, recv, device):
        return pltpu.make_async_remote_copy(
            src_ref=src, dst_ref=dst, send_sem=send, recv_sem=recv, device_id=device, device_id_type=MESH
        )

    def f_piece(ref, p, t):
        return ref.at[:, pl.ds(pl.multiple_of(p * rows + t * rq, rq), rq), :]

    def f_send(p, t, device, own=False):
        src = f_ref.at[:, pl.ds(pl.multiple_of(t * rq, rq), rq), :] if own else f_piece(fall, p, t)
        remote(src, f_piece(fall, p, t), fsend, frecv.at[p, t], device).start()

    def f_wait(p, t):
        remote(f_piece(fall, p, t), f_piece(fall, p, t), fsend, frecv.at[p, t], (me, q)).wait_recv()

    def w_piece(m, p):
        return wall.at[m, pl.ds(pl.multiple_of(p * rows, rows), rows), :]

    def w_own(m, p):
        remote(wsrc.at[m], w_piece(m, me), wsend, wrecv.at[m, me], (p, q)).start()

    def w_wait(m, p):
        remote(w_piece(m, p), w_piece(m, p), wsend, wrecv.at[m, p], (me, q)).wait_recv()

    def w_forward(m, p):
        w_wait(m, p)
        remote(w_piece(m, p), w_piece(m, p), wsend, wrecv.at[m, p], (y_peer, q)).start()

    for p in z_peers:
        f_send(me, q, (p, q), own=True)
    f_send(me, q, (y_peer, q), own=True)

    wsrc[0] = wq_ref[...].astype(BF)
    wsrc[1] = wk_ref[...].astype(BF)
    wsrc[2] = wo_ref[...].T.astype(BF)
    for p in z_peers:
        w_own(0, p)
    keeps = []
    for m in range(3):
        keep = pltpu.make_async_copy(wsrc.at[m], w_piece(m, me), own_sem.at[m])
        keep.start()
        keeps.append(keep)
    fall[:, pl.ds(pl.multiple_of(me * rows, rows), rows), :] = f_ref[...]

    def share(p, t, stage):
        for bit in bits[stage:]:
            f_send(p, t, (me, flip(q, bit)))

    def from_z(p):
        f_wait(p, q)
        f_send(p, q, (y_peer, q))
        share(p, q, 0)

    def from_y(p):
        f_wait(p, q)
        share(p, q, 0)

    tasks = [functools.partial(from_z, p) for p in z_peers]
    tasks.append(functools.partial(from_y, y_peer))
    work = []
    for m in range(3):
        for c in range(CHUNKS):
            work.append((m, c))
    per_task = max(1, -(-len(tasks) // 6))
    lhs = [gq_ref, gk_ref, ao_ref]
    left = None
    for step, (m, c) in enumerate(work):
        if c == 0:
            left = lhs[m][...].T
        a = 0 if m < 2 else 1
        if m != 1:
            loads[a * CHUNKS + c].wait()
        cut = slice(c * width, (c + 1) * width)
        gt[m, :, cut] = jnp.dot(left, xv[a, :, cut], preferred_element_type=F32).astype(BF)
        if step >= 5:
            for task in tasks[:per_task]:
                task()
            tasks = tasks[per_task:]
    for task in tasks:
        task()
    for m in range(3):
        w_own(m, y_peer)
    for p in z_peers:
        w_own(1, p)
    for p in y_side:
        from_y(p)
    held = [q]
    for stage, bit in enumerate(bits):
        arriving = [flip(t, bit) for t in held]
        for p in others:
            for t in arriving:
                f_wait(p, t)
                share(p, t, stage + 1)
        held = held + arriving
    keep_f = pltpu.make_async_copy(fall, fall_out, own_sem.at[3])
    keep_f.start()

    for m in range(3):
        projected = jnp.dot(gt[m], fall[m], preferred_element_type=F32).T
        ps[:, m] = projected.reshape(n, rk, projected.shape[1]).astype(BF)
    for p in others:
        remote(ps.at[p], pr.at[me], psend, precv.at[me], (p, q)).start()
    pr[me] = ps[me]
    for p in z_peers:
        w_own(2, p)
    for p in z_peers:
        w_forward(0, p)
    for p in others:
        remote(pr.at[p], pr.at[p], psend, precv.at[p], (me, q)).wait_recv()
    reduced = pr[0].astype(F32)
    for i in range(1, n):
        reduced = reduced + pr[i].astype(F32)
    first_new = first_decay * m1_ref[...] + (1.0 - first_decay) * reduced
    second_new = second_decay * m2_ref[...] + (1.0 - second_decay) * reduced * reduced
    ratio = first_new / (jnp.sqrt(second_new) + epsilon)
    rsrc[...] = ratio.astype(BF)
    part[...] = jnp.broadcast_to(jnp.sum(ratio * ratio).reshape(1, 1), part.shape)
    for p in z_peers + [y_peer]:
        remote(rsrc, rall.at[me], rsend, rrecv.at[me], (p, q)).start()
    for k, t in enumerate(tp_peers):
        remote(part, parts_tp.at[q], tsend.at[k], trecv.at[q], (me, t)).start()
    first_ref[...] = first_new
    second_ref[...] = second_new
    rall[me] = rsrc[...]
    parts_tp[q] = part[...]
    for t in tp_peers:
        remote(part, parts_tp.at[t], tsend.at[0], trecv.at[t], (me, q)).wait_recv()
    total = parts_tp[0]
    for t in range(1, ntp):
        total = total + parts_tp[t]
    psum_fs[...] = total
    for k, p in enumerate(others):
        remote(psum_fs, parts_fs.at[me], ssend.at[k], srecv.at[me], (p, q)).start()
    parts_fs[me] = total

    def r_wait(p):
        remote(rall.at[p], rall.at[p], rsend, rrecv.at[p], (me, q)).wait_recv()

    for p in z_peers:
        r_wait(p)
        remote(rall.at[p], rall.at[p], rsend, rrecv.at[p], (y_peer, q)).start()
    for m in (1, 2):
        for p in z_peers:
            w_forward(m, p)
    for p in [y_peer] + y_side:
        r_wait(p)
    for m in range(3):
        r_out[m] = rall[:, m].astype(F32).reshape(r_out.shape[1], r_out.shape[2]).astype(BF)
    for p in others:
        remote(psum_fs, parts_fs.at[p], ssend.at[0], srecv.at[p], (me, q)).wait_recv()
    square_total = parts_fs[0]
    for i in range(1, n):
        square_total = square_total + parts_fs[i]
    count = 3 * (rk * n) * (m1_ref.shape[2] * ntp)
    scale_out[...] = lax.rsqrt(square_total / count + 1.0)

    for m in range(3):
        for p in [y_peer] + y_side:
            w_wait(m, p)
    for keep in keeps:
        keep.wait()
    keep_f.wait()
    span = fall.at[:, pl.ds(0, (n - 1) * rows), :]
    remote(span, span, fsend, frecv.at[0, 0], (me, q)).wait_send()
    span = wall.at[:, pl.ds(0, (n - 1) * rows), :]
    remote(span, span, wsend, wrecv.at[0, 0], (me, q)).wait_send()
    span = ps.at[pl.ds(0, n - 1)]
    remote(span, span, psend, precv.at[0], (me, q)).wait_send()
    span = rall.at[pl.ds(0, n - 1)]
    remote(span, span, rsend, rrecv.at[0], (me, q)).wait_send()
    for k, t in enumerate(tp_peers):
        remote(part, part, tsend.at[k], trecv.at[0], (me, q)).wait_send()
    for k, p in enumerate(others):
        remote(psum_fs, psum_fs, ssend.at[k], srecv.at[0], (me, q)).wait_send()


def per_device(
    n, ntp,
    inputs, attn_out, grad_query, grad_key, grad_mixed, query_weight, key_weight, out_weight,
    factors, moment_first, moment_second,
):
    tokens, depth = inputs.shape
    cols = grad_query.shape[1]
    rows, rank = factors.shape[1:]
    rk = moment_first.shape[1]
    anyspace = pl.BlockSpec(memory_space=pl.ANY)
    vmem = pl.BlockSpec(memory_space=pltpu.VMEM)
    dma = pltpu.SemaphoreType.DMA
    shape = jax.ShapeDtypeStruct
    fall, wall, directions, scale, first_new, second_new = pl.pallas_call(
        functools.partial(kernel, n, ntp),
        out_shape=(
            shape((3, depth, rank), BF),
            shape((3, depth, cols), BF),
            shape((3, rank, cols), BF),
            shape((1, 128), F32),
            shape(moment_first.shape, F32),
            shape(moment_second.shape, F32),
        ),
        in_specs=[anyspace] * 2 + [vmem] * 9,
        out_specs=(anyspace, anyspace, vmem, vmem, vmem, vmem),
        scratch_shapes=[
            pltpu.VMEM((2, tokens, depth), BF),
            pltpu.VMEM((3, cols, depth), BF),
            pltpu.VMEM((3, depth, rank), BF),
            pltpu.VMEM((3, rows, cols), BF),
            pltpu.VMEM((n, 3, rk, cols), BF),
            pltpu.VMEM((n, 3, rk, cols), BF),
            pltpu.VMEM((3, rk, cols), BF),
            pltpu.VMEM((n, 3, rk, cols), BF),
            pltpu.VMEM((1, 128), F32),
            pltpu.VMEM((ntp, 1, 128), F32),
            pltpu.VMEM((1, 128), F32),
            pltpu.VMEM((n, 1, 128), F32),
            dma((2 * CHUNKS,)), dma((4,)),
            dma, dma((n, ntp)), dma, dma((3, n)), dma, dma((n,)), dma, dma((n,)),
            dma((n,)), dma((n,)), dma((ntp,)), dma((ntp,)),
        ],
        compiler_params=pltpu.CompilerParams(
            collective_id=0, has_side_effects=True, vmem_limit_bytes=60 * 1024 * 1024
        ),
    )(
        inputs, grad_mixed, grad_query, grad_key, attn_out, query_weight, key_weight, out_weight,
        factors, moment_first, moment_second,
    )
    step_scale = scale[0, 0]

    def product(left, number):
        return jnp.dot(left, directions[number], preferred_element_type=F32)

    step_query = step_scale * product(factors[0], 0)
    step_key = step_scale * product(factors[1], 1)
    step_out = step_scale * product(factors[2], 2).T
    rate = learn_rate * step_scale
    copies = [
        (wall[m].astype(F32) - rate * product(fall[m], m)).astype(BF) for m in range(3)
    ]
    return (step_query, step_key, step_out, copies[0], copies[1], copies[2].T, first_new, second_new)


def solution(mesh):
    in_specs = (
        P("fs", None),
        P("fs", "tp"),
        P("fs", "tp"),
        P("fs", "tp"),
        P("fs", None),
        P("fs", "tp"),
        P("fs", "tp"),
        P("tp", "fs"),
        P(None, "fs", None),
        P(None, "fs", "tp"),
        P(None, "fs", "tp"),
    )
    out_specs = (
        P("fs", "tp"),
        P("fs", "tp"),
        P("tp", "fs"),
        P(None, "tp"),
        P(None, "tp"),
        P("tp", None),
        P(None, "fs", "tp"),
        P(None, "fs", "tp"),
    )
    return jax.shard_map(
        functools.partial(per_device, mesh.shape["fs"], mesh.shape["tp"]),
        mesh=mesh, in_specs=in_specs, out_specs=out_specs, check_vma=False,
    )
```

time: 358 us -> 101 us (0.28)
  waiting for transfers between devices: 246 us -> 0 us
  Pallas kernels: 0 us -> 85.3 us
  blocking collectives: 68.8 us -> 0 us
  between operations: 14.7 us -> 1.33 us
  matrix products: 16.7 us -> 9.5 us
  local copies, waits for them, and re-layouts: 8.36 us -> 4.4 us
    all_gather x4 -> x0, waiting for transfers between devices: 183 us -> none  [the longest x1 65 us: per_device(): whole_factors = lax.all_gather(factors, 'fs', axis=1, tiled=True)]
    pallas_call x0 -> x1, Pallas kernels: none -> 85.3 us  [per_device(): pl.pallas_call(functools.partial(kernel, n, ntp), out_shape=(shape((3, de...]
    reduce_scatter x1 -> x0, waiting for transfers between devices: 62.6 us -> none  [per_device(): lax.psum_scatter(partial_sums, 'fs', scatter_dimension=1, tiled=True)]
    psum x1 -> x0, blocking collectives: 37.6 us -> none  [per_device(): square_total = lax.psum(jnp.sum(adam_ratio * adam_ratio), ('fs', 'tp'))]
    all_gather x1 -> x0, blocking collectives: 31.2 us -> none  [per_device(): lax.all_gather(adam_ratio.astype(jnp.bfloat16), 'fs', axis=1, tiled=True)]
    dot_general x12 -> x6, matrix products: 16.7 us -> 9.5 us  [product(): return jnp.dot(left, directions[number], preferred_element_type=F32)]
    unnamed x39 -> x15, local copies, waits for them, and re-layouts: 8.36 us -> 4.4 us
  transfers between devices with their start and end apart: 5 -> 0, of which waited for: 5 -> 0; matrix products, arithmetic and copies ran while one was open for 2% -> 0% of each run, Pallas kernels for 0% -> 0%
where the time goes in v1:
time: 101 us
  Pallas kernels  85.3 us (84%)
  matrix products  9.5 us (9%)
  local copies, waits for them, and re-layouts  4.4 us (4%)
  between operations  1.33 us (1%)
    pallas_call x1, Pallas kernels, per_device(): pl.pallas_call(functools.partial(kernel, n, ntp), out_shape=(shape((3, de...  85.3 us
    dot_general x6, matrix products, product(): return jnp.dot(left, directions[number], preferred_element_type=F32)  9.5 us
    unnamed x15, local copies, waits for them, and re-layouts  4.4 us

profile of v1, /device:TPU:0, one launch (start us, length us, event | category | flops | bytes accessed | tf_op | source)
XLA Modules:
  0.0 100.5 jit_solution(13178492709184467968)
XLA Ops:
  0.6 85.3 %shard_map.170 = (bf16[3,2048,256]{2,1,0:T(8,128)(2,1)}, bf16[3,2048,256]{2,1,0:T(8,128)(2,1)}, bf16[3,256,256]{2,1,0:T(8,128)(2,1)}, f32[1,128]{1,0:T(1,128)}, ...) custom-call(bf16[2048,2048]{1,0:T(8,128)(2,1)} %x_hbm.1, bf16[2048,2048]{1,0:T(8,128)(2,1)} %mixed_hbm.1, ...), custom_call_target="tpu_custom_call" | custom-call | tf_op jit(solution)/shard_map/pallas_call | solution.py:255
  86.6 0.0 copy-start.1
  86.6 2.1 %fusion.6 = bf16[256,2048]{0,1:T(8,128)(2,1)S(1)} fusion(bf16[3,2048,256]{2,1,0:T(8,128)(2,1)} %get-tuple-element.17, bf16[3,2048,256]{2,1,0:T(8,128)(2,1)} %get-tuple-element.16, f32[]{:T(128)S(6)} %mul_shard_map.3, bf16[3,256,256]{2,1,0:T(8,128)(2,1)} %get-tuple-element.15), kind=kOutput, calls=%fused_computation.9 | convolution fusion | flops 270532608 | bytes 3276804 | tf_op jit(solution)/shard_map/dot_general | solution.py:294
  88.7 1.4 %copy.21 = bf16[256,2048]{1,0:T(8,128)(2,1)} copy(bf16[256,2048]{0,1:T(8,128)(2,1)S(1)} %fusion.6) | data formatting | bytes 2097152
  90.1 0.0 copy-done.1
  90.1 2.9 %fusion.4 = bf16[2048,256]{1,0:T(8,128)(2,1)} fusion(bf16[3,2048,256]{2,1,0:T(8,128)(2,1)} %get-tuple-element.17, bf16[3,2048,256]{2,1,0:T(8,128)(2,1)} %get-tuple-element.16, f32[]{:T(128)S(6)} %mul_shard_map.3, bf16[3,256,256]{2,1,0:T(8,128)(2,1)S(1)} %copy-done.1), kind=kOutput, calls=%fused_computation.7 | convolution fusion | flops 270532608 | bytes 3276804 | tf_op jit(solution)/shard_map/dot_general | solution.py:294
  93.0 0.0 copy-start
  93.0 0.0 copy-start.4
  93.0 3.0 %fusion.3 = bf16[2048,256]{1,0:T(8,128)(2,1)} fusion(bf16[3,2048,256]{2,1,0:T(8,128)(2,1)} %get-tuple-element.17, f32[]{:T(128)S(6)} %mul_shard_map.3, bf16[3,2048,256]{2,1,0:T(8,128)(2,1)} %get-tuple-element.16, bf16[3,256,256]{2,1,0:T(8,128)(2,1)S(1)} %copy-done.1), kind=kOutput, calls=%fused_computation.6 | convolution fusion | flops 270532608 | bytes 3276804 | tf_op jit(solution)/shard_map/dot_general | solution.py:294
  96.0 0.0 copy-done
  96.0 0.0 copy-done.4
  96.1 0.0 copy-start.3
  96.1 0.0 copy-start.2
  96.1 1.0 convolution_multiply_fusion.3
  97.0 0.3 fusion.7
  97.3 0.8 copy.20
  98.1 0.3 fusion.8
  98.4 0.8 copy.19
  99.2 0.0 copy-done.3
  99.2 0.6 copy.24
  99.9 0.0 copy-done.2
  99.9 0.6 copy.25
Async XLA Ops:
  86.6 3.5 %copy-start.1 = (bf16[3,256,256]{2,1,0:T(8,128)(2,1)S(1)}, bf16[3,256,256]{2,1,0:T(8,128)(2,1)}, u32[]{:S(2)}) copy-start(bf16[3,256,256]{2,1,0:T(8,128)(2,1)} %get-tuple-element.15) | copy-start | bytes 1179652
  93.0 3.0 %copy-start = (bf16[3,256,256]{2,1,0:T(8,128)(2,1)S(1)}, bf16[3,256,256]{2,1,0:T(8,128)(2,1)}, u32[]{:S(2)}) copy-start(bf16[3,256,256]{2,1,0:T(8,128)(2,1)} %f_ref.1) | copy-start | bytes 1179652
  93.0 3.0 %copy-start.4 = (f32[1,128]{1,0:T(1,128)S(1)}, f32[1,128]{1,0:T(1,128)}, u32[]{:S(2)}) copy-start(f32[1,128]{1,0:T(1,128)} %get-tuple-element.14) | copy-start | bytes 1540
  96.1 3.2 %copy-start.3 = (f32[3,32,256]{2,1,0:T(8,128)S(1)}, f32[3,32,256]{2,1,0:T(8,128)}, u32[]{:S(2)}) copy-start(f32[3,32,256]{2,1,0:T(8,128)} %get-tuple-element.42) | copy-start | bytes 294916
  96.1 3.8 %copy-start.2 = (f32[3,32,256]{2,1,0:T(8,128)S(1)}, f32[3,32,256]{2,1,0:T(8,128)}, u32[]{:S(2)}) copy-start(f32[3,32,256]{2,1,0:T(8,128)} %get-tuple-element.43) | copy-start | bytes 294916
